TPU v7x, 256 devices: a whole 4x4x8 slice. The times are simulated.
256 devices in a mesh: rep: 2 (over z_hi), fs: 16 (over z_lo, x), tp: 8 (over y, core).
Axes of the slice: x: 4, y: 4, z: 8 (z_hi: 2, z_lo: 4; z = z_hi * 4 + z_lo), core: 2. Of those that a mesh axis runs over, the one named last changes fastest.
Arguments:
- stream: bfloat16 [32768, 2048], P(('rep', 'fs', 'tp')), may hold values from -6 to 6
- gate_weight: bfloat16 [2048, 2816], P('fs', 'tp'), may hold values from -0.125 to 0.125
- up_weight: bfloat16 [2048, 2816], P('fs', 'tp'), may hold values from -0.125 to 0.125
- down_weight: bfloat16 [2816, 2048], P('tp', 'fs'), may hold values from -0.21875 to 0.21875
- query_weight: bfloat16 [2048, 512], P('fs', 'tp'), may hold values from -0.125 to 0.125
- key_weight: bfloat16 [2048, 512], P('fs', 'tp'), may hold values from -0.125 to 0.125
- value_weight: bfloat16 [2048, 1024], P('fs', 'tp'), may hold values from -0.125 to 0.125
- outgate_weight: bfloat16 [2048, 1024], P('fs', 'tp'), may hold values from -0.125 to 0.125
- decay_down: bfloat16 [2048, 32], replicated, may hold values from -0.125 to 0.125
- decay_up: bfloat16 [32, 512], P(None, 'tp'), may hold values from -2 to 2
- decay_bias: float32 [512], P('tp'), may hold values from -0.5 to 7
- head_gain: float32 [128], replicated, may hold values from 0.1 to 1.9
- out_weight: bfloat16 [1024, 2048], P('tp', 'fs'), may hold values from -0.375 to 0.375
- norm_gain: float32 [3, 2048], replicated, may hold values from 0.1 to 1.9
Outputs:
- layer_out: bfloat16 [32768, 2048], P(('rep', 'fs', 'tp'))
All inputs are finite; a program needn't handle non-finite values.
Results may differ from a plain program's by a relative error of at most 0.015.
Values may be sent and summed in bfloat16 or wider, within the bound.
A program may use at most 128 MiB of HBM per device.

v0:
```python
import jax
import jax.numpy as jnp
from jax import lax
from jax.sharding import PartitionSpec as P

DK = 64
DV = 128
BLOCK = 64
RESIDUAL_SCALE = 2.0**0.5
BRANCH_SCALE = 0.5
NORM_EPS = 1e-05
HEAD_EPS = 0.01
GATE_DIVISOR = 16.0


def from_everyone(value, axis):
    copies = jnp.broadcast_to(value, (lax.axis_size(axis), *value.shape))
    return lax.all_to_all(copies, axis, split_axis=0, concat_axis=0, tiled=True)


def joined_along(pieces, dim):
    pieces = jnp.moveaxis(pieces, 0, dim)
    lengths = pieces.shape
    return pieces.reshape(*lengths[:dim], lengths[dim] * lengths[dim + 1], *lengths[dim + 2 :])


def gather_directly(value, axis, dim):
    pieces = from_everyone(value, axis)
    return joined_along(pieces, dim)


def side_by_side(arrays, axis, dim, along):
    widths = [a.shape[along] for a in arrays]
    both = jnp.concatenate(arrays, axis=along)
    result = lax.all_gather(both, axis, axis=dim, tiled=True)
    return tuple(jnp.split(result, [sum(widths[:k]) for k in range(1, len(widths))], axis=along))


def layer_norm(values, norm_scale):
    average = jnp.mean(values, -1, keepdims=True)
    centred = values - average
    spread = jnp.mean(centred * centred, -1, keepdims=True)
    return (centred * lax.rsqrt(spread + NORM_EPS) * norm_scale).astype(jnp.bfloat16)


def blocked_mixer(query, key_rows, value_rows, log_gate):
    length, head_count, key_dim = query.shape
    value_dim = value_rows.shape[2]
    block_count = length // BLOCK

    def split_blocks(values):
        return values.reshape(block_count, BLOCK, head_count, values.shape[2]).transpose(0, 2, 1, 3)

    causal = jnp.tril(jnp.ones((BLOCK, BLOCK), dtype=bool))

    def advance(carried, inputs):
        query_blk, key_blk, value_blk, decay_blk = inputs
        log_gaps = decay_blk[:, :, None, :] - decay_blk[:, None, :, :]
        log_gaps = jnp.where(causal[None, :, :, None], log_gaps, -jnp.inf)
        scores = jnp.sum(
            query_blk[:, :, None, :] * key_blk[:, None, :, :] * jnp.exp(log_gaps), axis=-1
        )
        inside = jnp.einsum("hij,hjv->hiv", scores, value_blk)
        carried_part = jnp.einsum("hid,hdv->hiv", query_blk * jnp.exp(decay_blk), carried)
        closing = decay_blk[:, -1, :]
        update = jnp.einsum(
            "hjd,hjv->hdv", key_blk * jnp.exp(closing[:, None, :] - decay_blk), value_blk
        )
        return (carried * jnp.exp(closing)[:, :, None] + update, inside + carried_part)

    cumulative = jnp.cumsum(split_blocks(log_gate), axis=2)
    start_state = jnp.zeros((head_count, key_dim, value_dim), jnp.float32)
    _, outputs = lax.scan(
        advance,
        start_state,
        (split_blocks(query), split_blocks(key_rows), split_blocks(value_rows), cumulative),
    )
    return outputs.transpose(0, 2, 1, 3).reshape(length, head_count, value_dim)


def on_device(
    stream,
    gate_weight,
    up_weight,
    down_weight,
    query_weight,
    key_weight,
    value_weight,
    outgate_weight,
    decay_down,
    decay_up,
    decay_bias,
    head_gain,
    out_weight,
    norm_gain,
):
    down_local = gather_directly(down_weight, "fs", 1)
    down_full = lax.all_gather(down_local, "tp", axis=0, tiled=True)

    def ffn_half(current, norm_scale):
        gathered = lax.all_gather(current, "tp", axis=0, tiled=True)
        pieces = side_by_side((gate_weight, up_weight), "fs", 0, 1)
        gate = jnp.dot(gathered, pieces[0], preferred_element_type=jnp.float32)
        upward = jnp.dot(gathered, pieces[1], preferred_element_type=jnp.float32)
        hidden = (jax.nn.silu(gate) * upward).astype(jnp.bfloat16)
        own_hidden = lax.all_to_all(hidden, "tp", split_axis=0, concat_axis=1, tiled=True)
        summed = jnp.dot(own_hidden, down_full, preferred_element_type=jnp.float32)
        return layer_norm(
            RESIDUAL_SCALE * current.astype(jnp.float32) + BRANCH_SCALE * summed, norm_scale
        )

    first = ffn_half(stream, norm_gain[0])
    gathered = lax.all_gather(first, "tp", axis=0, tiled=True)
    length = gathered.shape[0]
    pieces = side_by_side((query_weight, key_weight, value_weight, outgate_weight), "fs", 0, 1)
    query, key_rows, value_rows, outgate = tuple(
        (jnp.dot(gathered, piece, preferred_element_type=jnp.float32) for piece in pieces)
    )
    query = query.astype(jnp.bfloat16)
    key_rows = key_rows.astype(jnp.bfloat16)
    value_rows = value_rows.astype(jnp.bfloat16)
    outgate = outgate.astype(jnp.bfloat16)
    low_rank = jnp.dot(gathered, decay_down, preferred_element_type=jnp.float32).astype(
        jnp.bfloat16
    )
    pre_gate = jnp.dot(low_rank, decay_up, preferred_element_type=jnp.float32) + decay_bias
    log_gate = jax.nn.log_sigmoid(pre_gate) / GATE_DIVISOR
    local_heads = query.shape[1] // DK
    mixed = blocked_mixer(
        query.astype(jnp.float32).reshape(length, local_heads, DK) * DK ** (-0.5),
        key_rows.astype(jnp.float32).reshape(length, local_heads, DK),
        value_rows.astype(jnp.float32).reshape(length, local_heads, DV),
        log_gate.reshape(length, local_heads, DK),
    )
    normed = mixed * lax.rsqrt(jnp.mean(mixed * mixed, -1, keepdims=True) + HEAD_EPS) * head_gain
    gated = (
        normed.reshape(length, local_heads * DV) * jax.nn.silu(outgate.astype(jnp.float32))
    ).astype(jnp.bfloat16)
    out_local = gather_directly(out_weight, "fs", 1)
    out_full = lax.all_gather(out_local, "tp", axis=0, tiled=True)
    own_gated = lax.all_to_all(gated, "tp", split_axis=0, concat_axis=1, tiled=True)
    summed = jnp.dot(own_gated, out_full, preferred_element_type=jnp.float32)
    second = layer_norm(RESIDUAL_SCALE * first.astype(jnp.float32) + summed, norm_gain[1])
    return ffn_half(second, norm_gain[2])


def solution(mesh):
    in_specs = (
        P(("rep", "fs", "tp"), None),
        P("fs", "tp"),
        P("fs", "tp"),
        P("tp", "fs"),
        P("fs", "tp"),
        P("fs", "tp"),
        P("fs", "tp"),
        P("fs", "tp"),
        P(),
        P(None, "tp"),
        P("tp"),
        P(),
        P("tp", "fs"),
        P(),
    )
    out_specs = P(("rep", "fs", "tp"), None)
    return jax.shard_map(
        on_device, mesh=mesh, in_specs=in_specs, out_specs=out_specs, check_vma=False
    )
```

profile of v0, /device:TPU:1, one launch (start us, length us, event | category | flops | bytes accessed | tf_op | source)
XLA Modules:
  0.0 473.2 jit_solution(7399616951409170826)
XLA Ops:
  6.5 1.7 pad_maximum_fusion
  8.3 0.7 all-gather.10.cloned.1.call-update
  9.0 1.1 broadcast_in_dim.32
  10.1 57.1 %all_to_all.67 = bf16[16,352,128]{2,1,0:T(8,128)(2,1)S(1)} all-to-all(bf16[16,352,128]{2,1,0:T(8,128)(2,1)S(1)} %broadcast_in_dim.32), channel_id=1, replica_groups=mesh['rep'=2,'fs'=16,'tp'=8] {'fs'}, dimensions={0} | all-to-all | bytes 2883584 | tf_op jit(solution)/shard_map/all_to_all | solution.py:18
  67.2 1.3 copy_bitcast_fusion
  68.9 0.7 pad_maximum_fusion.1
  69.6 27.4 %all-gather.8.cloned.1.call-done = bf16[2048,704]{0,1:T(8,128)(2,1)} async-done(((bf16[128,704]{0,1:T(8,128)(2,1)}), bf16[2048,704]{0,1:T(8,128)(2,1)}) %all-gather.8.cloned.1.call-update) | async-done | bytes 2883600 | tf_op jit(solution)/shard_map/all_gather | solution.py:35
  97.0 44.9 %all-gather.10.cloned.1.call-done = bf16[1024,2048]{1,0:T(8,128)(2,1)} async-done(((bf16[128,2048]{1,0:T(8,128)(2,1)}), bf16[1024,2048]{1,0:T(8,128)(2,1)}) %all-gather.10.cloned.1.call-update) | async-done | bytes 4194320 | tf_op jit(solution)/shard_map/all_gather | solution.py:101
  141.9 4.5 convolution_bitcast_fusion.2
  146.4 1.9 fusion.35
  148.3 1.0 copy.67
  149.3 3.7 all-to-all-start
  153.1 14.9 %all-to-all-done = bf16[8,128,352]{1,2,0:T(8,128)(2,1)S(1)} async-done(((bf16[8,128,352]{1,2,0:T(8,128)(2,1)}), bf16[8,128,352]{1,2,0:T(8,128)(2,1)S(1)}, u32[]{:S(2)}, u32[]{:S(2)}) %all-to-all-start) | async-done | bytes 720928 | tf_op jit(solution)/shard_map/all_to_all | solution.py:106
  168.0 45.3 %all-gather.12.cloned.1.call-done = bf16[2816,2048]{1,0:T(8,128)(2,1)} async-done(((bf16[352,2048]{1,0:T(8,128)(2,1)}), bf16[2816,2048]{1,0:T(8,128)(2,1)}) %all-gather.12.cloned.1.call-update) | async-done | bytes 11534352 | tf_op jit(solution)/shard_map/all_gather | solution.py:98
  213.3 6.0 %fusion.58 = (f32[128]{0:T(128)S(1)}, f32[128,2048]{1,0:T(8,128)S(1)}) fusion(bf16[128,2816]{0,1:T(8,128)(2,1)S(1)} %bitcast.148, bf16[2816,2048]{1,0:T(8,128)(2,1)} %all-gather.12.cloned.1.call-done, bf16[128,2048]{1,0:T(8,128)(2,1)S(1)} %copy-done.3), kind=kOutput, calls=%fused_computation.96 | convolution fusion | flops 1477705600 | bytes 13828608 | tf_op jit(solution)/shard_map/dot_general | solution.py:107
  219.3 0.3 multiply_reduce_fusion.3
  219.6 1.0 multiply_convert_fusion.2
  220.8 0.9 broadcast_in_dim.35
  221.7 7.0 %all-to-all-start.3 = ((bf16[16,128,128]{1,2,0:T(8,128)(2,1)}), bf16[16,128,128]{1,2,0:T(8,128)(2,1)S(1)}, u32[]{:S(2)}, u32[]{:S(2)}) async-start(bf16[16,128,128]{1,2,0:T(8,128)(2,1)} %broadcast_in_dim.35), calls=%async_computation.3 | async-start | bytes 1048576 | tf_op jit(solution)/shard_map/all_to_all | solution.py:18
  228.8 0.2 all-gather.18.cloned.1.call-start
  229.0 17.3 %all-to-all-done.3 = bf16[16,128,128]{1,2,0:T(8,128)(2,1)S(1)} async-done(((bf16[16,128,128]{1,2,0:T(8,128)(2,1)}), bf16[16,128,128]{1,2,0:T(8,128)(2,1)S(1)}, u32[]{:S(2)}, u32[]{:S(2)}) %all-to-all-start.3) | async-done | bytes 524320 | tf_op jit(solution)/shard_map/all_to_all | solution.py:18
  246.3 0.9 copy-done.4
  247.2 39.2 %all-gather.16.cloned.1.call-done = bf16[2048,384]{1,0:T(8,128)(2,1)} async-done(((bf16[128,384]{1,0:T(8,128)(2,1)}), bf16[2048,384]{1,0:T(8,128)(2,1)}) %all-gather.16.cloned.1.call-update) | async-done | bytes 1572880 | tf_op jit(solution)/shard_map/all_gather | solution.py:35
  286.4 45.3 %all-gather.14.cloned.1.call-done = bf16[1024,2048]{1,0:T(8,128)(2,1)} async-done(((bf16[128,2048]{1,0:T(8,128)(2,1)}), bf16[1024,2048]{1,0:T(8,128)(2,1)}) %all-gather.14.cloned.1.call-update) | async-done | bytes 4194320 | tf_op jit(solution)/shard_map/all_gather | solution.py:113
  331.8 3.8 fusion.45
  335.5 0.2 copy.57
  335.7 3.7 fusion.44
  339.5 0.2 copy.58
  339.7 3.8 fusion.56
  343.6 0.4 copy.47
  344.0 6.3 %fusion.61 = f32[16,1,64,64]{3,0,1,2:T(8,128)S(1)} fusion(f32[16,1,64,64]{3,0,1,2:T(8,128)S(1)} %copy.47), kind=kOutput, calls=%fused_computation.99 | output fusion | flops 4128768 | bytes 524288 | tf_op jit(solution)/shard_map/jit(cumsum)/reduce_window_sum | solution.py:71
  350.3 3.6 convolution_convert_fusion.1
  353.9 30.5 %while.13 = (s32[]{:T(128)}, f32[1,64,128]{2,1,0:T(8,128)S(1)}, f32[16,1,64,128]{3,2,1,0:T(8,128)S(1)}, f32[16,1,64,64]{3,0,1,2:T(8,128)S(1)}, f32[16,1,64,64]{3...) while((s32[]{:T(128)}, f32[1,64,128]{2,1,0:T(8,128)S(1)}, ...), condition=%wide.region_5.6_spmd.clone, body=%wide.region_3.5_spmd.clone.sunk | while | flops 4509699 | bytes 544884 | solution.py:73
  354.0 1.4 multiply_reduce_fusion.6
  355.9 1.4 multiply_reduce_fusion.6
  357.8 1.4 multiply_reduce_fusion.6
  359.7 1.4 multiply_reduce_fusion.6
  361.6 1.4 multiply_reduce_fusion.6
  363.5 1.4 multiply_reduce_fusion.6
  365.4 1.4 multiply_reduce_fusion.6
  367.3 1.4 multiply_reduce_fusion.6
  369.2 1.4 multiply_reduce_fusion.6
  371.1 1.4 multiply_reduce_fusion.6
  373.0 1.4 multiply_reduce_fusion.6
  374.9 1.4 multiply_reduce_fusion.6
  376.8 1.4 multiply_reduce_fusion.6
  378.7 1.4 multiply_reduce_fusion.6
  380.6 1.4 multiply_reduce_fusion.6
  382.6 1.4 multiply_reduce_fusion.6
  384.4 0.2 multiply_reduce_fusion.4
  384.7 3.6 fusion.52
  388.3 0.9 copy.54
  389.2 3.6 all-to-all-start.2
  392.8 6.5 %all-to-all-done.2 = bf16[8,128,128]{1,2,0:T(8,128)(2,1)S(1)} async-done(((bf16[8,128,128]{1,2,0:T(8,128)(2,1)}), bf16[8,128,128]{1,2,0:T(8,128)(2,1)S(1)}, u32[]{:S(2)}, u32[]{:S(2)}) %all-to-all-start.2) | async-done | bytes 262176 | tf_op jit(solution)/shard_map/all_to_all | solution.py:141
  399.3 3.8 fusion.59
  403.0 0.3 multiply_reduce_fusion.2
  403.3 1.0 multiply_convert_fusion.1
  404.4 35.0 %all-gather.20.cloned.1.call-done = bf16[1024,2048]{1,0:T(8,128)(2,1)} async-done(((bf16[128,2048]{1,0:T(8,128)(2,1)}), bf16[1024,2048]{1,0:T(8,128)(2,1)}) %all-gather.20.cloned.1.call-update) | async-done | bytes 4194320 | tf_op jit(solution)/shard_map/all_gather | solution.py:101
  439.3 4.5 fusion.38
  443.8 4.6 fusion.34
  448.6 14.7 %all_to_all.68 = bf16[8,128,352]{1,2,0:T(8,128)(2,1)S(1)} all-to-all(bf16[8,128,352]{1,2,0:T(8,128)(2,1)S(1)} %bitcast.150), channel_id=1, replica_groups=mesh['rep'=2,'fs'=16,'tp'=8] {'tp'}, dimensions={0} | all-to-all | bytes 1441792 | tf_op jit(solution)/shard_map/all_to_all | solution.py:106
  463.3 1.8 fusion.60
  465.1 0.3 multiply_reduce_fusion.1
  465.3 1.0 multiply_convert_fusion
  (195 shorter events, 9.2 us)
Async XLA Ops:
  6.5 333.1 %copy-start = (bf16[2048,32]{0,1:T(8,128)(2,1)S(1)}, bf16[2048,32]{0,1:T(8,128)(2,1)}, u32[]{:S(2)}) copy-start(bf16[2048,32]{0,1:T(8,128)(2,1)} %param.24) | copy-start | bytes 393220
  6.5 90.5 %all-gather.8.cloned.1.call-start = ((), (), s32[]{:S(2)}) async-start(), calls=%async_computation.5 | async-start | bytes 3063808 | tf_op jit(solution)/shard_map/all_gather | solution.py:35
  8.2 133.7 %all-gather.10.cloned.1.call-start = ((), (), s32[]{:S(2)}) async-start(), calls=%async_computation.6 | async-start | bytes 4718592 | tf_op jit(solution)/shard_map/all_gather | solution.py:101
  9.0 204.3 %all-gather.12.cloned.1.call-start = ((), (), s32[]{:S(2)}) async-start(), calls=%async_computation.7 | async-start | bytes 12976128 | tf_op jit(solution)/shard_map/all_gather | solution.py:98
  67.2 1.4 copy-start.9
  67.2 1.5 copy-start.10
  67.2 1.6 copy-start.5
  67.2 1.6 copy-start.6
  68.6 217.8 %all-gather.16.cloned.1.call-start = ((), (), s32[]{:S(2)}) async-start(), calls=%async_computation.9 | async-start | bytes 1671168 | tf_op jit(solution)/shard_map/all_gather | solution.py:35
  97.0 49.4 %copy-start.14 = (bf16[2048,704]{0,1:T(8,128)(2,1)S(1)}, bf16[2048,704]{0,1:T(8,128)(2,1)}, u32[]{:S(2)}) copy-start(bf16[2048,704]{0,1:T(8,128)(2,1)} %all-gather.8.cloned.1.call-done) | copy-start | bytes 8650756
  141.9 4.5 copy-start.13
  148.3 4.8 %copy-start.8 = (f32[3,2048]{1,0:T(4,128)S(1)}, f32[3,2048]{1,0:T(4,128)}, u32[]{:S(2)}) copy-start(f32[3,2048]{1,0:T(4,128)} %param.29) | copy-start | bytes 73732
  148.3 64.9 %copy-start.3 = (bf16[128,2048]{1,0:T(8,128)(2,1)S(1)}, bf16[128,2048]{1,0:T(8,128)(2,1)}, u32[]{:S(2)}) copy-start(bf16[128,2048]{1,0:T(8,128)(2,1)} %param.16) | copy-start | bytes 1572868
  149.3 18.6 %all-to-all-start = ((bf16[8,128,352]{1,2,0:T(8,128)(2,1)}), bf16[8,128,352]{1,2,0:T(8,128)(2,1)S(1)}, u32[]{:S(2)}, u32[]{:S(2)}) async-start(bf16[8,128,352]{1,2,0:T(8,128)(2,1)} %bitcast.112), calls=%async_computation | async-start | bytes 1441792 | tf_op jit(solution)/shard_map/all_to_all | solution.py:106
  153.1 178.7 %all-gather.14.cloned.1.call-start = ((), (), s32[]{:S(2)}) async-start(), calls=%async_computation.8 | async-start | bytes 4718592 | tf_op jit(solution)/shard_map/all_gather | solution.py:113
  219.3 1.3 copy-start.7
  221.7 24.6 %all-to-all-start.3 = ((bf16[16,128,128]{1,2,0:T(8,128)(2,1)}), bf16[16,128,128]{1,2,0:T(8,128)(2,1)S(1)}, u32[]{:S(2)}, u32[]{:S(2)}) async-start(bf16[16,128,128]{1,2,0:T(8,128)(2,1)} %broadcast_in_dim.35), calls=%async_computation.3 | async-start | bytes 1048576 | tf_op jit(solution)/shard_map/all_to_all | solution.py:18
  228.8 164.0 %all-gather.18.cloned.1.call-start = ((), (), s32[]{:S(2)}) async-start(), calls=%async_computation.10 | async-start | bytes 4718592 | tf_op jit(solution)/shard_map/all_gather | solution.py:140
  246.3 0.9 copy-start.4
  335.7 4.0 copy-start.11
  335.7 4.0 copy-start.12
  353.9 30.8 %copy-start.15 = (f32[128]{0:T(128)S(1)}, f32[128]{0:T(128)}, u32[]{:S(2)}) copy-start(f32[128]{0:T(128)} %param.27) | copy-start | bytes 1540
  384.7 14.6 %copy-start.1 = (bf16[128,2048]{1,0:T(8,128)(2,1)S(1)}, bf16[128,2048]{1,0:T(8,128)(2,1)}, u32[]{:S(2)}) copy-start(bf16[128,2048]{1,0:T(8,128)(2,1)} %multiply_convert_fusion.2) | copy-start | bytes 1572868
  389.2 10.1 %all-to-all-start.2 = ((bf16[8,128,128]{1,2,0:T(8,128)(2,1)}), bf16[8,128,128]{1,2,0:T(8,128)(2,1)S(1)}, u32[]{:S(2)}, u32[]{:S(2)}) async-start(bf16[8,128,128]{1,2,0:T(8,128)(2,1)} %copy.54), calls=%async_computation.2 | async-start | bytes 524288 | tf_op jit(solution)/shard_map/all_to_all | solution.py:141
  392.8 46.6 %all-gather.20.cloned.1.call-start = ((), (), s32[]{:S(2)}) async-start(), calls=%async_computation.11 | async-start | bytes 4718592 | tf_op jit(solution)/shard_map/all_gather | solution.py:101
  439.3 23.9 %slice-start = ((s8[11534336]{0:T(1024)(128)(4,1)}), s8[4194304]{0:T(1024)(128)(4,1)S(1)}, s32[]{:S(2)}) async-start(s8[11534336]{0:T(1024)(128)(4,1)} %bitcast.141), calls=%async_computation.12 | async-start | bytes 8388608
  439.3 23.9 %slice-start.1 = ((s8[11534336]{0:T(1024)(128)(4,1)}), s8[4194304]{0:T(1024)(128)(4,1)S(1)}, s32[]{:S(2)}) async-start(s8[11534336]{0:T(1024)(128)(4,1)} %bitcast.141), calls=%async_computation.13 | async-start | bytes 8388608
  443.8 19.5 %slice-start.2 = ((s8[11534336]{0:T(1024)(128)(4,1)}), s8[3145728]{0:T(1024)(128)(4,1)S(1)}, s32[]{:S(2)}) async-start(s8[11534336]{0:T(1024)(128)(4,1)} %bitcast.141), calls=%async_computation.14 | async-start | bytes 6291456
  448.4 14.8 %copy-start.2 = (bf16[128,2048]{1,0:T(8,128)(2,1)S(1)}, bf16[128,2048]{1,0:T(8,128)(2,1)}, u32[]{:S(2)}) copy-start(bf16[128,2048]{1,0:T(8,128)(2,1)} %multiply_convert_fusion.1) | copy-start | bytes 1572868
Sparse Core Ops, SparseCore 0:
  9.0 87.9 all-gather.7
  98.9 42.9 all-gather.9
  143.8 69.4 all-gather.11
  214.9 71.4 all-gather.15
  288.1 43.5 all-gather.13
  333.4 38.1 all-gather.17
  404.5 34.8 all-gather.19
where the time goes:
time: 474 us; the launch traced here: 473 us
  waiting for transfers between devices  277 us (58%)
  blocking collectives  71.8 us (15%)
  matrix products  52.6 us (11%)
  other arithmetic  34.7 us (7%)
  starting transfers between devices  14.7 us (3%)
  between operations  13.8 us (3%)
  local copies, waits for them, and re-layouts  8.37 us (2%)
    all_gather x2, waiting for transfers between devices, ffn_half(): gathered = lax.all_gather(current, 'tp', axis=0, tiled=True)  79.9 us
    all_gather x2, waiting for transfers between devices, side_by_side(): result = lax.all_gather(both, axis, axis=dim, tiled=True)  66.6 us
    all_to_all x1, blocking collectives, from_everyone(): return lax.all_to_all(copies, axis, split_axis=0, concat_axis=0, tiled=True)  57.1 us
    all_gather x1, waiting for transfers between devices, on_device(): gathered = lax.all_gather(first, 'tp', axis=0, tiled=True)  45.3 us
    all_gather x1, waiting for transfers between devices, on_device(): down_full = lax.all_gather(down_local, 'tp', axis=0, tiled=True)  45.3 us
    reduce_sum x16, other arithmetic, advance(): jnp.sum(query_blk[:, :, None, :] * key_blk[:, None, :, :] * jnp.exp(log_g...  21.7 us
    all_to_all x1, waiting for transfers between devices, from_everyone(): return lax.all_to_all(copies, axis, split_axis=0, concat_axis=0, tiled=True)  17.3 us
    all_to_all x1, waiting for transfers between devices, ffn_half(): lax.all_to_all(hidden, 'tp', split_axis=0, concat_axis=1, tiled=True)  14.9 us
  transfers between devices with their start and end apart: 10, of which 9 were waited for; matrix products, arithmetic and copies ran while one was open for 16% of the time, Pallas kernels for 0%

commit v1 on v0

--- a/solution.py
+++ b/solution.py
@@ -11,6 +11,15 @@
 NORM_EPS = 1e-05
 HEAD_EPS = 0.01
 GATE_DIVISOR = 16.0
+
+
+def define_things_on_mesh(local, which_dim):
+    local = jnp.moveaxis(local, 0, which_dim)
+    y_new = local.shape
+    next_value = local.reshape(
+        *y_new[:which_dim], y_new[which_dim] * y_new[which_dim + 1], *y_new[which_dim + 2 :]
+    )
+    return next_value
 
 
 def from_everyone(value, axis):
@@ -95,7 +104,23 @@
     norm_gain,
 ):
     down_local = gather_directly(down_weight, "fs", 1)
-    down_full = lax.all_gather(down_local, "tp", axis=0, tiled=True)
+    degree = lax.axis_size("tp")
+    line_up = tuple(((u, (u + 1) % degree) for u in range(degree)))
+    ledger = tuple(((c, kk) for kk, c in line_up))
+    out_arr, seen_now = ([], [])
+    for dd in range(degree - 1):
+        if dd % 2 == 0:
+            out_arr.append(
+                lax.ppermute(out_arr[-1] if out_arr else down_local, perm=line_up, axis_name="tp")
+            )
+        else:
+            seen_now.append(
+                lax.ppermute(seen_now[-1] if seen_now else down_local, axis_name="tp", perm=ledger)
+            )
+    aux = jnp.stack([*out_arr[::-1], down_local, *seen_now])
+    odd = lax.axis_index("tp") - len(out_arr)
+    aux = aux[(jnp.arange(degree) - odd) % degree]
+    down_full = define_things_on_mesh(aux, 0)
 
     def ffn_half(current, norm_scale):
         gathered = lax.all_gather(current, "tp", axis=0, tiled=True)

time: 474 us -> 447 us (0.943)
  blocking collectives: 71.8 us -> 14.7 us
  waiting for transfers between devices: 277 us -> 229 us
  starting transfers between devices: 14.7 us -> 61.9 us
  local copies, waits for them, and re-layouts: 8.37 us -> 39.6 us
    all_to_all x1 -> x0, blocking collectives: 57.1 us -> none  [from_everyone(): return lax.all_to_all(copies, axis, split_axis=0, concat_axis=0, tiled=True)]
    ppermute x0 -> x7, waiting for transfers between devices: none -> 46.6 us  [the longest x4 46.6 us: on_device(): lax.ppermute(out_arr[-1] if out_arr else down_local, perm=line_up, axis_n...]
    all_gather x1 -> x0, waiting for transfers between devices: 45.3 us -> none  [on_device(): down_full = lax.all_gather(down_local, 'tp', axis=0, tiled=True)]
    all_to_all x1 -> x2, waiting for transfers between devices: 17.3 us -> 51.4 us  [from_everyone(): return lax.all_to_all(copies, axis, split_axis=0, concat_axis=0, tiled=True)]
    all_gather x1, waiting for transfers between devices: 45.3 us -> 12.7 us  [on_device(): gathered = lax.all_gather(first, 'tp', axis=0, tiled=True)]
    all_gather x2, waiting for transfers between devices: 79.9 us -> 49.6 us  [ffn_half(): gathered = lax.all_gather(current, 'tp', axis=0, tiled=True)]
    ppermute x0 -> x7, starting transfers between devices: none -> 24.6 us  [the longest x4 15.6 us: on_device(): lax.ppermute(out_arr[-1] if out_arr else down_local, perm=line_up, axis_n...]
    unnamed x43 -> x62, local copies, waits for them, and re-layouts: 1.67 us -> 18.6 us
  transfers between devices with their start and end apart: 10 -> 17, of which waited for: 9 -> 10; matrix products, arithmetic and copies ran while one was open for 16% -> 22% of each run, Pallas kernels for 0% -> 0%
where the time goes in v1:
time: 447 us; the launch traced here: 446 us
  waiting for transfers between devices  229 us (51%)
  starting transfers between devices  61.9 us (14%)
  matrix products  51.7 us (12%)
  local copies, waits for them, and re-layouts  39.6 us (9%)
  other arithmetic  34.7 us (8%)
  blocking collectives  14.7 us (3%)
  between operations  13.9 us (3%)
    all_gather x2, waiting for transfers between devices, side_by_side(): result = lax.all_gather(both, axis, axis=dim, tiled=True)  61.6 us
    all_to_all x2, waiting for transfers between devices, from_everyone(): return lax.all_to_all(copies, axis, split_axis=0, concat_axis=0, tiled=True)  51.4 us
    all_gather x2, waiting for transfers between devices, ffn_half(): gathered = lax.all_gather(current, 'tp', axis=0, tiled=True)  49.6 us
    ppermute x4, waiting for transfers between devices, on_device(): lax.ppermute(out_arr[-1] if out_arr else down_local, perm=line_up, axis_n...  46.6 us
    reduce_sum x16, other arithmetic, advance(): jnp.sum(query_blk[:, :, None, :] * key_blk[:, None, :, :] * jnp.exp(log_g...  21.7 us
    unnamed x62, local copies, waits for them, and re-layouts  18.6 us
    all_to_all x2, starting transfers between devices, from_everyone(): return lax.all_to_all(copies, axis, split_axis=0, concat_axis=0, tiled=True)  17.5 us
    all_to_all x1, starting transfers between devices, on_device(): lax.all_to_all(gated, 'tp', split_axis=0, concat_axis=1, tiled=True)  15.8 us
  transfers between devices with their start and end apart: 17, of which 10 were waited for; matrix products, arithmetic and copies ran while one was open for 22% of the time, Pallas kernels for 0%

profile of v1, /device:TPU:1, one launch (start us, length us, event | category | flops | bytes accessed | tf_op | source)
XLA Modules:
  0.0 446.2 jit_solution(5728296789005256240)
XLA Ops:
  6.5 1.7 pad_maximum_fusion
  8.2 2.2 broadcast_in_dim.32
  10.4 9.1 %all-to-all-start.1 = ((bf16[16,352,128]{2,1,0:T(8,128)(2,1)}), bf16[16,352,128]{2,1,0:T(8,128)(2,1)S(1)}, u32[]{:S(2)}, u32[]{:S(2)}) async-start(bf16[16,352,128]{2,1,0:T(8,128)(2,1)} %broadcast_in_dim.32), calls=%async_computation.1 | async-start | bytes 2883584 | tf_op jit(solution)/shard_map/all_to_all | solution.py:27
  20.3 37.4 %all-to-all-done.1 = bf16[16,352,128]{2,1,0:T(8,128)(2,1)S(1)} async-done(((bf16[16,352,128]{2,1,0:T(8,128)(2,1)}), bf16[16,352,128]{2,1,0:T(8,128)(2,1)S(1)}, u32[]{:S(2)}, u32[]{:S(2)}) %all-to-all-start.1) | async-done | bytes 1441824 | tf_op jit(solution)/shard_map/all_to_all | solution.py:27
  57.9 8.0 %collective-permute-start = (bf16[352,2048]{1,0:T(8,128)(2,1)S(1)}, bf16[352,2048]{1,0:T(8,128)(2,1)S(1)}, u32[]{:S(2)}, u32[]{:S(2)}) collective-permute-start(bf16[352,2048]{1,0:T(8,128)(2,1)S(1)} %copy_bitcast_fusion), channel_id=1, source_target_pairs={{0,1},{1,2},{2,3},{3,4},{4,5},{5,6},{6,7},{7,0},{8,9},{9,10},{10,1... | collective-permute-start | bytes 4325384 | tf_op jit(solution)/shard_map/ppermute | solution.py:114
  66.0 16.0 %collective-permute-done = bf16[352,2048]{1,0:T(8,128)(2,1)S(1)} collective-permute-done((bf16[352,2048]{1,0:T(8,128)(2,1)S(1)}, bf16[352,2048]{1,0:T(8,128)(2,1)S(1)}, u32[]{:S(2)}, u32[]{:S(2)}) %collective-permute-start) | collective-permute-done | bytes 1441824 | tf_op jit(solution)/shard_map/ppermute | solution.py:114
  81.9 1.1 copy-done.6
  83.0 2.5 collective-permute-start.1
  85.5 15.9 %collective-permute-done.1 = bf16[352,2048]{1,0:T(8,128)(2,1)S(1)} collective-permute-done((bf16[352,2048]{1,0:T(8,128)(2,1)S(1)}, bf16[352,2048]{1,0:T(8,128)(2,1)S(1)}, u32[]{:S(2)}, u32[]{:S(2)}) %collective-permute-start.1) | collective-permute-done | bytes 1441824 | tf_op jit(solution)/shard_map/ppermute | solution.py:114
  101.5 1.1 copy-done.8
  102.6 2.5 collective-permute-start.2
  105.0 1.2 collective-permute-start.5
  106.3 14.7 %collective-permute-done.2 = bf16[352,2048]{1,0:T(8,128)(2,1)} collective-permute-done((bf16[352,2048]{1,0:T(8,128)(2,1)S(1)}, bf16[352,2048]{1,0:T(8,128)(2,1)}, u32[]{:S(2)}, u32[]{:S(2)}) %collective-permute-start.2) | collective-permute-done | bytes 1441824 | tf_op jit(solution)/shard_map/ppermute | solution.py:114
  121.0 2.6 collective-permute-start.3
  124.9 7.8 %collective-permute-start.6 = (bf16[352,2048]{1,0:T(8,128)(2,1)}, bf16[352,2048]{1,0:T(8,128)(2,1)}, u32[]{:S(2)}, u32[]{:S(2)}) collective-permute-start(bf16[352,2048]{1,0:T(8,128)(2,1)} %collective-permute-done.5), channel_id=1, source_target_pairs={{1,0},{2,1},{3,2},{4,3},{5,4},{6,5},{7,6},{0,7},{9,8},{10,9},{11,1... | collective-permute-start | bytes 4325384 | tf_op jit(solution)/shard_map/ppermute | solution.py:118
  132.6 17.4 %all-gather.9.cloned.1.call-done = bf16[1024,2048]{1,0:T(8,128)(2,1)} async-done(((bf16[128,2048]{1,0:T(8,128)(2,1)}), bf16[1024,2048]{1,0:T(8,128)(2,1)}) %all-gather.9.cloned.1.call-update) | async-done | bytes 4194320 | tf_op jit(solution)/shard_map/all_gather | solution.py:126
  150.0 4.5 convolution_bitcast_fusion.4
  154.8 1.8 fusion.37
  157.7 3.7 all-to-all-start
  161.4 2.8 bitcast_dynamic-update-slice_fusion.6
  164.2 2.7 bitcast_dynamic-update-slice_fusion.5
  166.9 1.2 bitcast_dynamic-update-slice_fusion.4
  168.2 1.2 bitcast_dynamic-update-slice_fusion.3
  169.4 1.2 constant_dynamic-update-slice_fusion
  170.6 2.6 bitcast_dynamic-update-slice_fusion.2
  173.2 2.6 bitcast_dynamic-update-slice_fusion.1
  175.9 2.7 bitcast_dynamic-update-slice_fusion
  178.5 10.4 %gather_fusion = bf16[8,352,2048]{2,1,0:T(8,128)(2,1)} fusion(bf16[8,352,2048]{2,1,0:T(8,128)(2,1)} %bitcast_dynamic-update-slice_fusion, s32[1024]{0:T(1024)S(1)} %pad_clamp_fusion), kind=kCustom, calls=%fused_computation | custom fusion | bytes 23068704 | tf_op jit(solution)/shard_map/gather | solution.py:122
  188.9 6.0 %fusion.64 = (f32[128]{0:T(128)S(1)}, f32[128,2048]{1,0:T(8,128)S(1)}) fusion(bf16[8,352,2048]{2,1,0:T(8,128)(2,1)} %gather_fusion, bf16[8,128,352]{1,2,0:T(8,128)(2,1)S(1)} %all-to-all-done, bf16[128,2048]{1,0:T(8,128)(2,1)S(1)} %copy-done.5), kind=kOutput, calls=%fused_computation.116 | convolution fusion | flops 1477705600 | bytes 13828608 | tf_op jit(solution)/shard_map/dot_general | solution.py:132
  198.5 8.4 %all-to-all-start.3 = ((bf16[16,128,128]{1,2,0:T(8,128)(2,1)}), bf16[16,128,128]{1,2,0:T(8,128)(2,1)S(1)}, u32[]{:S(2)}, u32[]{:S(2)}) async-start(bf16[16,128,128]{1,2,0:T(8,128)(2,1)} %broadcast_in_dim.35), calls=%async_computation.3 | async-start | bytes 1048576 | tf_op jit(solution)/shard_map/all_to_all | solution.py:27
  207.1 14.0 %all-to-all-done.3 = bf16[16,128,128]{1,2,0:T(8,128)(2,1)S(1)} async-done(((bf16[16,128,128]{1,2,0:T(8,128)(2,1)}), bf16[16,128,128]{1,2,0:T(8,128)(2,1)S(1)}, u32[]{:S(2)}, u32[]{:S(2)}) %all-to-all-start.3) | async-done | bytes 524320 | tf_op jit(solution)/shard_map/all_to_all | solution.py:27
  222.0 12.7 %all-gather.11.cloned.1.call-done = bf16[1024,2048]{1,0:T(8,128)(2,1)} async-done(((bf16[128,2048]{1,0:T(8,128)(2,1)}), bf16[1024,2048]{1,0:T(8,128)(2,1)}) %all-gather.11.cloned.1.call-update) | async-done | bytes 4194320 | tf_op jit(solution)/shard_map/all_gather | solution.py:138
  234.7 3.8 fusion.60
  239.0 6.3 %fusion.67 = f32[16,1,64,64]{3,0,1,2:T(8,128)S(1)} fusion(f32[16,1,64,64]{3,0,1,2:T(8,128)S(1)} %copy.51), kind=kOutput, calls=%fused_computation.119 | output fusion | flops 4128768 | bytes 524288 | tf_op jit(solution)/shard_map/jit(cumsum)/reduce_window_sum | solution.py:80
  245.3 61.6 %all-gather.13.cloned.1.call-done = bf16[2048,384]{1,0:T(8,128)(2,1)} async-done(((bf16[128,384]{1,0:T(8,128)(2,1)}), bf16[2048,384]{1,0:T(8,128)(2,1)}) %all-gather.13.cloned.1.call-update) | async-done | bytes 1572880 | tf_op jit(solution)/shard_map/all_gather | solution.py:44
  306.9 3.8 fusion.47
  310.9 3.7 fusion.46
  314.8 3.6 convolution_convert_fusion.1
  318.4 30.5 %while.13 = (s32[]{:T(128)}, f32[1,64,128]{2,1,0:T(8,128)S(1)}, f32[16,1,64,128]{3,2,1,0:T(8,128)S(1)}, f32[16,1,64,64]{3,0,1,2:T(8,128)S(1)}, f32[16,1,64,64]{3...) while((s32[]{:T(128)}, f32[1,64,128]{2,1,0:T(8,128)S(1)}, ...), condition=%wide.region_5.6_spmd.clone, body=%wide.region_3.5_spmd.clone.sunk | while | flops 4509699 | bytes 544884 | solution.py:82
  318.4 1.4 multiply_reduce_fusion.6
  320.3 1.4 multiply_reduce_fusion.6
  322.3 1.4 multiply_reduce_fusion.6
  324.2 1.4 multiply_reduce_fusion.6
  326.1 1.4 multiply_reduce_fusion.6
  328.0 1.4 multiply_reduce_fusion.6
  329.9 1.4 multiply_reduce_fusion.6
  331.8 1.4 multiply_reduce_fusion.6
  333.7 1.4 multiply_reduce_fusion.6
  335.6 1.4 multiply_reduce_fusion.6
  337.5 1.4 multiply_reduce_fusion.6
  339.4 1.4 multiply_reduce_fusion.6
  341.3 1.4 multiply_reduce_fusion.6
  343.2 1.4 multiply_reduce_fusion.6
  345.1 1.4 multiply_reduce_fusion.6
  347.0 1.4 multiply_reduce_fusion.6
  349.2 3.6 fusion.56
  353.7 15.8 %all-to-all-start.2 = ((bf16[8,128,128]{1,2,0:T(8,128)(2,1)}), bf16[8,128,128]{1,2,0:T(8,128)(2,1)S(1)}, u32[]{:S(2)}, u32[]{:S(2)}) async-start(bf16[8,128,128]{1,2,0:T(8,128)(2,1)} %copy.58), calls=%async_computation.2 | async-start | bytes 524288 | tf_op jit(solution)/shard_map/all_to_all | solution.py:166
  369.4 6.5 %all-to-all-done.2 = bf16[8,128,128]{1,2,0:T(8,128)(2,1)S(1)} async-done(((bf16[8,128,128]{1,2,0:T(8,128)(2,1)}), bf16[8,128,128]{1,2,0:T(8,128)(2,1)S(1)}, u32[]{:S(2)}, u32[]{:S(2)}) %all-to-all-start.2) | async-done | bytes 262176 | tf_op jit(solution)/shard_map/all_to_all | solution.py:166
  375.9 3.8 fusion.65
  381.0 32.2 %all-gather.17.cloned.1.call-done = bf16[1024,2048]{1,0:T(8,128)(2,1)} async-done(((bf16[128,2048]{1,0:T(8,128)(2,1)}), bf16[1024,2048]{1,0:T(8,128)(2,1)}) %all-gather.17.cloned.1.call-update) | async-done | bytes 4194320 | tf_op jit(solution)/shard_map/all_gather | solution.py:126
  413.2 4.0 fusion.40
  417.3 4.2 fusion.36
  421.6 14.7 %all_to_all.61 = bf16[8,128,352]{1,2,0:T(8,128)(2,1)S(1)} all-to-all(bf16[8,128,352]{1,2,0:T(8,128)(2,1)S(1)} %bitcast.179), channel_id=1, replica_groups=mesh['rep'=2,'fs'=16,'tp'=8] {'tp'}, dimensions={0} | all-to-all | bytes 1441792 | tf_op jit(solution)/shard_map/all_to_all | solution.py:131
  436.3 1.8 fusion.66
  (232 shorter events, 21.0 us)
Async XLA Ops:
  6.5 228.2 %copy-start = (bf16[2048,32]{0,1:T(8,128)(2,1)S(1)}, bf16[2048,32]{0,1:T(8,128)(2,1)}, u32[]{:S(2)}) copy-start(bf16[2048,32]{0,1:T(8,128)(2,1)} %param.24) | copy-start | bytes 393220
  6.5 126.1 %all-gather.7.cloned.1.call-start = ((), (), s32[]{:S(2)}) async-start(), calls=%async_computation.5 | async-start | bytes 3063808 | tf_op jit(solution)/shard_map/all_gather | solution.py:44
  10.4 113.2 %copy-start.13 = (f32[3,2048]{1,0:T(4,128)S(1)}, f32[3,2048]{1,0:T(4,128)}, u32[]{:S(2)}) copy-start(f32[3,2048]{1,0:T(4,128)} %param.29) | copy-start | bytes 73732
  10.4 47.3 %all-to-all-start.1 = ((bf16[16,352,128]{2,1,0:T(8,128)(2,1)}), bf16[16,352,128]{2,1,0:T(8,128)(2,1)S(1)}, u32[]{:S(2)}, u32[]{:S(2)}) async-start(bf16[16,352,128]{2,1,0:T(8,128)(2,1)} %broadcast_in_dim.32), calls=%async_computation.1 | async-start | bytes 2883584 | tf_op jit(solution)/shard_map/all_to_all | solution.py:27
  19.6 130.5 %all-gather.9.cloned.1.call-start = ((), (), s32[]{:S(2)}) async-start(), calls=%async_computation.6 | async-start | bytes 4718592 | tf_op jit(solution)/shard_map/all_gather | solution.py:126
  57.9 24.0 %collective-permute-start = (bf16[352,2048]{1,0:T(8,128)(2,1)S(1)}, bf16[352,2048]{1,0:T(8,128)(2,1)S(1)}, u32[]{:S(2)}, u32[]{:S(2)}) collective-permute-start(bf16[352,2048]{1,0:T(8,128)(2,1)S(1)} %copy_bitcast_fusion), channel_id=1, source_target_pairs={{0,1},{1,2},{2,3},{3,4},{4,5},{5,6},{6,7},{7,0},{8,9},{9,10},{10,1... | collective-permute-start | bytes 4325384 | tf_op jit(solution)/shard_map/ppermute | solution.py:114
  81.9 1.1 copy-start.6
  83.0 18.4 %collective-permute-start.1 = (bf16[352,2048]{1,0:T(8,128)(2,1)S(1)}, bf16[352,2048]{1,0:T(8,128)(2,1)S(1)}, u32[]{:S(2)}, u32[]{:S(2)}) collective-permute-start(bf16[352,2048]{1,0:T(8,128)(2,1)S(1)} %collective-permute-done), channel_id=1, source_target_pairs={{0,1},{1,2},{2,3},{3,4},{4,5},{5,6},{6,7},{7,0},{8,9},{9,10},{10,1... | collective-permute-start | bytes 4325384 | tf_op jit(solution)/shard_map/ppermute | solution.py:114
  85.5 19.6 %collective-permute-start.4 = (bf16[352,2048]{1,0:T(8,128)(2,1)S(1)}, bf16[352,2048]{1,0:T(8,128)(2,1)}, u32[]{:S(2)}, u32[]{:S(2)}) collective-permute-start(bf16[352,2048]{1,0:T(8,128)(2,1)S(1)} %copy_bitcast_fusion), channel_id=1, source_target_pairs={{1,0},{2,1},{3,2},{4,3},{5,4},{6,5},{7,6},{0,7},{9,8},{10,9},{11,1... | collective-permute-start | bytes 4325384 | tf_op jit(solution)/shard_map/ppermute | solution.py:118
  101.5 1.1 copy-start.8
  102.6 18.4 %collective-permute-start.2 = (bf16[352,2048]{1,0:T(8,128)(2,1)S(1)}, bf16[352,2048]{1,0:T(8,128)(2,1)}, u32[]{:S(2)}, u32[]{:S(2)}) collective-permute-start(bf16[352,2048]{1,0:T(8,128)(2,1)S(1)} %collective-permute-done.1), channel_id=1, source_target_pairs={{0,1},{1,2},{2,3},{3,4},{4,5},{5,6},{6,7},{7,0},{8,9},{9,10},{10,1... | collective-permute-start | bytes 4325384 | tf_op jit(solution)/shard_map/ppermute | solution.py:114
  105.0 19.8 %collective-permute-start.5 = (bf16[352,2048]{1,0:T(8,128)(2,1)}, bf16[352,2048]{1,0:T(8,128)(2,1)}, u32[]{:S(2)}, u32[]{:S(2)}) collective-permute-start(bf16[352,2048]{1,0:T(8,128)(2,1)} %collective-permute-done.4), channel_id=1, source_target_pairs={{1,0},{2,1},{3,2},{4,3},{5,4},{6,5},{7,6},{0,7},{9,8},{10,9},{11,1... | collective-permute-start | bytes 4325384 | tf_op jit(solution)/shard_map/ppermute | solution.py:118
  121.0 40.4 %collective-permute-start.3 = (bf16[352,2048]{1,0:T(8,128)(2,1)}, bf16[352,2048]{1,0:T(8,128)(2,1)}, u32[]{:S(2)}, u32[]{:S(2)}) collective-permute-start(bf16[352,2048]{1,0:T(8,128)(2,1)} %collective-permute-done.2), channel_id=1, source_target_pairs={{0,1},{1,2},{2,3},{3,4},{4,5},{5,6},{6,7},{7,0},{8,9},{9,10},{10,1... | collective-permute-start | bytes 4325384 | tf_op jit(solution)/shard_map/ppermute | solution.py:114
  124.9 51.0 %collective-permute-start.6 = (bf16[352,2048]{1,0:T(8,128)(2,1)}, bf16[352,2048]{1,0:T(8,128)(2,1)}, u32[]{:S(2)}, u32[]{:S(2)}) collective-permute-start(bf16[352,2048]{1,0:T(8,128)(2,1)} %collective-permute-done.5), channel_id=1, source_target_pairs={{1,0},{2,1},{3,2},{4,3},{5,4},{6,5},{7,6},{0,7},{9,8},{10,9},{11,1... | collective-permute-start | bytes 4325384 | tf_op jit(solution)/shard_map/ppermute | solution.py:118
  150.0 4.5 %copy-start.18 = (bf16[1024,2048]{1,0:T(8,128)(2,1)S(1)}, bf16[1024,2048]{1,0:T(8,128)(2,1)}, u32[]{:S(2)}) copy-start(bf16[1024,2048]{1,0:T(8,128)(2,1)} %all-gather.9.cloned.1.call-done) | copy-start | bytes 12582916
  150.0 4.8 %copy-start.19 = (bf16[2048,704]{0,1:T(8,128)(2,1)S(1)}, bf16[2048,704]{0,1:T(8,128)(2,1)}, u32[]{:S(2)}) copy-start(bf16[2048,704]{0,1:T(8,128)(2,1)} %all-gather.7.cloned.1.call-done) | copy-start | bytes 8650756
  157.7 31.2 %all-to-all-start = ((bf16[8,128,352]{1,2,0:T(8,128)(2,1)}), bf16[8,128,352]{1,2,0:T(8,128)(2,1)S(1)}, u32[]{:S(2)}, u32[]{:S(2)}) async-start(bf16[8,128,352]{1,2,0:T(8,128)(2,1)} %bitcast.142), calls=%async_computation | async-start | bytes 1441792 | tf_op jit(solution)/shard_map/all_to_all | solution.py:131
  161.4 73.3 %all-gather.11.cloned.1.call-start = ((), (), s32[]{:S(2)}) async-start(), calls=%async_computation.7 | async-start | bytes 4718592 | tf_op jit(solution)/shard_map/all_gather | solution.py:138
  161.4 5.6 %copy-start.9 = (bf16[352,2048]{1,0:T(8,128)(2,1)S(1)}, bf16[352,2048]{1,0:T(8,128)(2,1)}, u32[]{:S(2)}) copy-start(bf16[352,2048]{1,0:T(8,128)(2,1)} %copy-done.8) | copy-start | bytes 4325380
  164.2 4.0 copy-start.7
  178.5 10.4 %copy-start.5 = (bf16[128,2048]{1,0:T(8,128)(2,1)S(1)}, bf16[128,2048]{1,0:T(8,128)(2,1)}, u32[]{:S(2)}) copy-start(bf16[128,2048]{1,0:T(8,128)(2,1)} %param.16) | copy-start | bytes 1572868
  195.0 1.4 copy-start.14
  195.0 1.6 copy-start.15
  195.0 1.7 copy-start.10
  195.0 1.7 copy-start.11
  195.0 2.4 copy-start.12
  195.0 39.7 %copy-start.16 = (bf16[32,64]{1,0:T(8,128)(2,1)S(1)}, bf16[32,64]{1,0:T(8,128)(2,1)}, u32[]{:S(2)}) copy-start(bf16[32,64]{1,0:T(8,128)(2,1)} %param.25) | copy-start | bytes 12292
  195.0 39.7 %copy-start.17 = (f32[64]{0:T(128)S(1)}, f32[64]{0:T(128)}, u32[]{:S(2)}) copy-start(f32[64]{0:T(128)} %param.26) | copy-start | bytes 772
  196.4 110.5 %all-gather.13.cloned.1.call-start = ((), (), s32[]{:S(2)}) async-start(), calls=%async_computation.8 | async-start | bytes 1671168 | tf_op jit(solution)/shard_map/all_gather | solution.py:44
  198.5 22.7 %all-to-all-start.3 = ((bf16[16,128,128]{1,2,0:T(8,128)(2,1)}), bf16[16,128,128]{1,2,0:T(8,128)(2,1)S(1)}, u32[]{:S(2)}, u32[]{:S(2)}) async-start(bf16[16,128,128]{1,2,0:T(8,128)(2,1)} %broadcast_in_dim.35), calls=%async_computation.3 | async-start | bytes 1048576 | tf_op jit(solution)/shard_map/all_to_all | solution.py:27
  206.9 162.5 %all-gather.15.cloned.1.call-start = ((), (), s32[]{:S(2)}) async-start(), calls=%async_computation.9 | async-start | bytes 4718592 | tf_op jit(solution)/shard_map/all_gather | solution.py:165
  221.2 0.8 copy-start.4
  318.3 30.8 %copy-start.21 = (f32[128]{0:T(128)S(1)}, f32[128]{0:T(128)}, u32[]{:S(2)}) copy-start(f32[128]{0:T(128)} %param.27) | copy-start | bytes 1540
  349.2 26.7 %copy-start.2 = (bf16[128,2048]{1,0:T(8,128)(2,1)S(1)}, bf16[128,2048]{1,0:T(8,128)(2,1)}, u32[]{:S(2)}) copy-start(bf16[128,2048]{1,0:T(8,128)(2,1)} %multiply_convert_fusion.2) | copy-start | bytes 1572868
  353.7 22.2 %all-to-all-start.2 = ((bf16[8,128,128]{1,2,0:T(8,128)(2,1)}), bf16[8,128,128]{1,2,0:T(8,128)(2,1)S(1)}, u32[]{:S(2)}, u32[]{:S(2)}) async-start(bf16[8,128,128]{1,2,0:T(8,128)(2,1)} %copy.58), calls=%async_computation.2 | async-start | bytes 524288 | tf_op jit(solution)/shard_map/all_to_all | solution.py:166
  369.4 43.8 %all-gather.17.cloned.1.call-start = ((), (), s32[]{:S(2)}) async-start(), calls=%async_computation.10 | async-start | bytes 4718592 | tf_op jit(solution)/shard_map/all_gather | solution.py:126
  379.7 33.5 %copy-start.20 = (bf16[2048,704]{0,1:T(8,128)(2,1)S(1)}, bf16[2048,704]{0,1:T(8,128)(2,1)}, u32[]{:S(2)}) copy-start(bf16[2048,704]{0,1:T(8,128)(2,1)} %all-gather.7.cloned.1.call-done) | copy-start | bytes 8650756
  413.2 23.0 %slice-start = ((s8[11534336]{0:T(1024)(128)(4,1)}), s8[4194304]{0:T(1024)(128)(4,1)S(1)}, s32[]{:S(2)}) async-start(s8[11534336]{0:T(1024)(128)(4,1)} %bitcast.171), calls=%async_computation.11 | async-start | bytes 8388608
  413.2 23.0 %slice-start.1 = ((s8[11534336]{0:T(1024)(128)(4,1)}), s8[4194304]{0:T(1024)(128)(4,1)S(1)}, s32[]{:S(2)}) async-start(s8[11534336]{0:T(1024)(128)(4,1)} %bitcast.171), calls=%async_computation.12 | async-start | bytes 8388608
  417.2 19.0 %slice-start.2 = ((s8[11534336]{0:T(1024)(128)(4,1)}), s8[3145728]{0:T(1024)(128)(4,1)S(1)}, s32[]{:S(2)}) async-start(s8[11534336]{0:T(1024)(128)(4,1)} %bitcast.171), calls=%async_computation.13 | async-start | bytes 6291456
  421.4 14.8 %copy-start.3 = (bf16[128,2048]{1,0:T(8,128)(2,1)S(1)}, bf16[128,2048]{1,0:T(8,128)(2,1)}, u32[]{:S(2)}) copy-start(bf16[128,2048]{1,0:T(8,128)(2,1)} %multiply_convert_fusion.1) | copy-start | bytes 1572868
  436.3 3.1 copy-start.1
Sparse Core Ops, SparseCore 0:
  9.0 88.9 all-gather.6
  99.9 50.0 all-gather.8
  196.5 38.1 all-gather.10
  236.4 70.4 all-gather.12
  308.6 47.8 all-gather.14
  381.1 32.0 all-gather.16
